TPU v7x, 32 devices: a whole 2x2x4 slice. The times are simulated.
32 devices in a mesh: sp: 8 (over z, x), tp: 4 (over y, core).
Axes of the slice: x: 2, y: 2, z: 4, core: 2. Of those that a mesh axis runs over, the one named last changes fastest.
Arguments:
- tokens: bfloat16 [4096, 4096], P(('sp', 'tp')), may hold values from -6 to 6
- lock_projector: bfloat16 [4096, 1024], P(None, 'tp'), may hold values from -0.01171875 to 0.01171875
- value_weight: bfloat16 [4096, 2048], P(None, 'tp'), may hold values from -0.0234375 to 0.0234375
- decay_weight: bfloat16 [4096, 1024], P(None, 'tp'), may hold values from -0.09375 to 0.09375
- decay_offset: float32 [1024], P('tp'), may hold values from -3.5 to 0
- fresh_question: bfloat16 [16, 64], P('tp'), may hold values from -6 to 6
Outputs:
- state_cache: bfloat16 [16, 64, 128], P('tp', 'sp')
- first_read: bfloat16 [16, 128], P('tp')
All inputs are finite; a program needn't handle non-finite values.
Results may differ from a plain program's by a relative error of at most 0.0034.
Values may be sent and summed in bfloat16 or wider, within the bound.
No kernel may reach another device: no remote copies, remote signals or barrier semaphores. Data moves between devices by JAX's collectives and lax.ppermute only.
A program may use at most 64 MiB of HBM per device.

v0:
```python
import math
import jax
import jax.numpy as jnp
from jax import lax
from jax.sharding import PartitionSpec as P

CUE_WIDTH = 64
DV = 128
decay_tau = 16.0


def carried_in(part, axis, combine, identity):
    count = lax.axis_size(axis)
    place = lax.axis_index(axis)
    ahead = count - 1 - place
    gathered = lax.all_gather(part, axis)
    state = jnp.zeros_like(part) + jnp.asarray(identity, part.dtype)

    def one(hop, state):
        source = count - 1 - hop
        return combine(state, lax.dynamic_index_in_dim(gathered, source, 0, False))

    return lax.fori_loop(0, ahead, one, state)


def add_logs(earlier, later_sum):
    return earlier + later_sum


def per_device(tokens, lock_projector, value_weight, decay_weight, decay_offset, fresh_question):
    key_cols = lock_projector.shape[1]
    value_cols = value_weight.shape[1]
    local_heads = key_cols // CUE_WIDTH
    combined = jnp.concatenate([lock_projector, value_weight, decay_weight], axis=1)
    projected = jnp.dot(
        lax.all_gather(tokens, "tp", axis=0, tiled=True),
        combined,
        preferred_element_type=jnp.float32,
    )
    span_rows = projected.shape[0]
    lock_vectors = projected[:, :key_cols].astype(jnp.bfloat16)
    value_rows = projected[:, key_cols : key_cols + value_cols].astype(jnp.bfloat16)
    decay_pre = projected[:, key_cols + value_cols :]
    length = span_rows * lax.axis_size("sp")
    log_decay = jax.nn.log_sigmoid(decay_pre + decay_offset[None, :] + math.log(length)) / decay_tau
    segment_overall = jnp.sum(log_decay, axis=0)
    later_total = carried_in(segment_overall, "sp", add_logs, jnp.zeros_like(segment_overall))
    after = (segment_overall + later_total)[None, :] - jnp.cumsum(log_decay, axis=0)
    weighted = (lock_vectors.astype(jnp.float32) * jnp.exp(after)).astype(jnp.bfloat16)
    lookup_probes = weighted.reshape(span_rows, local_heads, CUE_WIDTH)
    stored_contents = value_rows.reshape(span_rows, local_heads, DV)
    summands_list = jnp.einsum(
        "nyl,nyp->ylp", lookup_probes, stored_contents, preferred_element_type=jnp.float32
    )
    key_scale = CUE_WIDTH ** (-0.5)
    question_widened = fresh_question.astype(jnp.float32)
    row_span = CUE_WIDTH // lax.axis_size("sp")
    row_start = lax.axis_index("sp") * row_span
    recall_grid = lax.psum(summands_list, "sp")
    segment_lines = lax.dynamic_slice_in_dim(recall_grid, row_start, row_span, 1)
    attended_blend = key_scale * jnp.einsum(
        "qw,qwi->qi", question_widened, recall_grid, precision=lax.Precision.HIGHEST
    )
    state_cache = segment_lines.astype(jnp.bfloat16)
    first_read = attended_blend * lax.rsqrt(
        jnp.mean(attended_blend * attended_blend, axis=-1, keepdims=True) + 1.0
    )
    return (state_cache, first_read.astype(jnp.bfloat16))


def solution(mesh):
    in_specs = (
        P(("sp", "tp"), None),
        P(None, "tp"),
        P(None, "tp"),
        P(None, "tp"),
        P("tp"),
        P("tp", None),
    )
    out_specs = (P("tp", "sp", None), P("tp", None))
    return jax.shard_map(
        per_device, mesh=mesh, in_specs=in_specs, out_specs=out_specs, check_vma=False
    )
```

profile of v0, /device:TPU:0, one launch (start us, length us, event | category | flops | bytes accessed | tf_op | source)
XLA Modules:
  0.0 155.6 jit_solution(18224980167365922461)
XLA Ops:
  7.2 0.0 copy-start
  7.2 0.0 all-gather.4.cloned.1.call-start
  7.2 0.7 all-gather.4.cloned.1.call-update
  7.9 0.0 all-reduce.2.cloned.1.call-start
  8.0 0.0 copy-start.1
  8.0 38.8 %all-gather.4.cloned.1.call-done = bf16[512,4096]{1,0:T(8,128)(2,1)} async-done(((bf16[128,4096]{1,0:T(8,128)(2,1)}), bf16[512,4096]{1,0:T(8,128)(2,1)}) %all-gather.4.cloned.1.call-update) | async-done | bytes 4194320 | tf_op jit(solution)/shard_map/all_gather | solution.py:36
  46.8 8.3 %fusion.22 = (bf16[512,1024]{0,1:T(8,128)(2,1)S(1)}, f32[512,1024]{0,1:T(8,128)S(1)}) fusion(bf16[512,4096]{1,0:T(8,128)(2,1)} %all-gather.4.cloned.1.call-done, bf16[4096,256]{1,0:T(8,128)(2,1)} %param.11, bf16[4096,512]{1,0:T(8,128)(2,1)} %param.10, bf16[4096,256]{1,0:T(8,128)(2,1)} %param.9), kind=kOutput, calls=%fused_computation.31 | convolution fusion | flops 4320657408 | bytes 15728640 | tf_op jit(solution)/shard_map/dot_general | solution.py:35
  55.1 0.0 copy-done.1
  55.1 0.5 fusion.21
  55.6 20.5 %all-gather.1 = f32[8,1,256]{2,1,0:T(1,128)S(1)} all-gather(f32[1,1,256]{2,1,0:T(1,128)S(1)} %bitcast.54), channel_id=2, replica_groups=mesh['sp'=8,'tp'=4] {'sp'}, dimensions={0}, use_global_device_ids=true | all-gather | bytes 9216 | tf_op jit(solution)/shard_map/all_gather | solution.py:16
  76.1 0.3 while.12
  76.5 0.2 reshape.30
  76.7 0.2 copy.11
  76.9 0.1 fusion.23
  77.2 0.3 copy.12
  77.5 0.2 fusion.14
  77.6 1.0 fusion.24
  78.6 0.0 all-reduce.2.cloned.1.call-update
  78.6 67.0 %all-reduce.2.cloned.1.call-done = f32[4,64,128]{2,1,0:T(8,128)} async-done(((f32[4,64,128]{2,1,0:T(8,128)}), f32[4,64,128]{2,1,0:T(8,128)}) %all-reduce.2.cloned.1.call-update) | async-done | bytes 131088 | tf_op jit(solution)/shard_map/psum | solution.py:59
  145.6 0.0 copy-done
  145.6 1.1 fusion.17
  146.7 0.1 multiply_reduce_fusion
  146.8 0.6 multiply_convert_fusion
  147.5 1.3 dynamic-slice_convert_fusion
  (24 shorter events, 0.3 us)
Async XLA Ops:
  7.2 138.4 %copy-start = (bf16[4,64]{1,0:T(4,128)(2,1)S(1)}, bf16[4,64]{1,0:T(4,128)(2,1)}, u32[]{:S(2)}) copy-start(bf16[4,64]{1,0:T(4,128)(2,1)} %param.13) | copy-start | bytes 1540
  7.2 39.6 %all-gather.4.cloned.1.call-start = ((), (), s32[]{:S(2)}) async-start(), calls=%async_computation | async-start | bytes 5242880 | tf_op jit(solution)/shard_map/all_gather | solution.py:36
  7.9 137.7 %all-reduce.2.cloned.1.call-start = ((), (), s32[]{:S(2)}) async-start(), calls=%async_computation.1 | async-start | bytes 262144 | tf_op jit(solution)/shard_map/psum | solution.py:59
  8.0 47.1 %copy-start.1 = (f32[256]{0:T(256)S(1)}, f32[256]{0:T(256)}, u32[]{:S(2)}) copy-start(f32[256]{0:T(256)} %param.12) | copy-start | bytes 3076
Sparse Core Ops, SparseCore 0:
  9.5 37.1 all-gather.3
  78.7 66.8 all-reduce.1
where the time goes:
time: 156 us
  waiting for transfers between devices  106 us (68%)
  blocking collectives  20.5 us (13%)
  between operations  14.1 us (9%)
  matrix products  10.3 us (7%)
  local copies, waits for them, and re-layouts  2.13 us (1%)
  other arithmetic  1.74 us (1%)
    psum x1, waiting for transfers between devices, per_device(): recall_grid = lax.psum(summands_list, 'sp')  67 us
    all_gather x1, waiting for transfers between devices, per_device(): lax.all_gather(tokens, 'tp', axis=0, tiled=True)  38.8 us
    all_gather x1, blocking collectives, carried_in(): gathered = lax.all_gather(part, axis)  20.5 us
    dot_general x1, matrix products, per_device(): jnp.dot(lax.all_gather(tokens, 'tp', axis=0, tiled=True), combined, prefe...  8.32 us
  transfers between devices with their start and end apart: 2, of which 2 were waited for; matrix products, arithmetic and copies ran while one was open for 0% of the time, Pallas kernels for 0%

commit v1 on v0

--- a/solution.py
+++ b/solution.py
@@ -56,7 +56,7 @@
     question_widened = fresh_question.astype(jnp.float32)
     row_span = CUE_WIDTH // lax.axis_size("sp")
     row_start = lax.axis_index("sp") * row_span
-    recall_grid = lax.psum(summands_list, "sp")
+    recall_grid = jnp.sum(lax.all_gather(summands_list, "sp"), axis=0)
     segment_lines = lax.dynamic_slice_in_dim(recall_grid, row_start, row_span, 1)
     attended_blend = key_scale * jnp.einsum(
         "qw,qwi->qi", question_widened, recall_grid, precision=lax.Precision.HIGHEST

time: 156 us -> 125 us (0.80)
  waiting for transfers between devices: 106 us -> 76.2 us
    psum x1 -> x0, waiting for transfers between devices: 67 us -> none  [per_device(): recall_grid = lax.psum(summands_list, 'sp')]
    all_gather x0 -> x1, waiting for transfers between devices: none -> 36.8 us  [per_device(): recall_grid = jnp.sum(lax.all_gather(summands_list, 'sp'), axis=0)]
where the time goes in v1:
time: 125 us
  waiting for transfers between devices  76.2 us (61%)
  blocking collectives  20.5 us (16%)
  between operations  14.2 us (11%)
  matrix products  9.44 us (8%)
  other arithmetic  3.04 us (2%)
  local copies, waits for them, and re-layouts  1.42 us (1%)
    all_gather x1, waiting for transfers between devices, per_device(): lax.all_gather(tokens, 'tp', axis=0, tiled=True)  38.8 us
    all_gather x1, waiting for transfers between devices, per_device(): recall_grid = jnp.sum(lax.all_gather(summands_list, 'sp'), axis=0)  36.8 us
    all_gather x1, blocking collectives, carried_in(): gathered = lax.all_gather(part, axis)  20.5 us
    dot_general x1, matrix products, per_device(): jnp.dot(lax.all_gather(tokens, 'tp', axis=0, tiled=True), combined, prefe...  8.32 us
  transfers between devices with their start and end apart: 2, of which 2 were waited for; matrix products, arithmetic and copies ran while one was open for 0% of the time, Pallas kernels for 0%

profile of v1, /device:TPU:0, one launch (start us, length us, event | category | flops | bytes accessed | tf_op | source)
XLA Modules:
  0.0 125.1 jit_solution(5661596509455975459)
XLA Ops:
  7.2 0.0 copy-start
  7.2 0.0 all-gather.6.cloned.1.call-start
  7.2 0.7 all-gather.6.cloned.1.call-update
  7.9 0.0 all-gather.8.cloned.1.call-start
  8.0 0.0 copy-start.1
  8.0 38.8 %all-gather.6.cloned.1.call-done = bf16[512,4096]{1,0:T(8,128)(2,1)} async-done(((bf16[128,4096]{1,0:T(8,128)(2,1)}), bf16[512,4096]{1,0:T(8,128)(2,1)}) %all-gather.6.cloned.1.call-update) | async-done | bytes 4194320 | tf_op jit(solution)/shard_map/all_gather | solution.py:36
  46.8 8.3 %fusion.22 = (bf16[512,1024]{0,1:T(8,128)(2,1)S(1)}, f32[512,1024]{0,1:T(8,128)S(1)}) fusion(bf16[512,4096]{1,0:T(8,128)(2,1)} %all-gather.6.cloned.1.call-done, bf16[4096,256]{1,0:T(8,128)(2,1)} %param.11, bf16[4096,512]{1,0:T(8,128)(2,1)} %param.10, bf16[4096,256]{1,0:T(8,128)(2,1)} %param.9), kind=kOutput, calls=%fused_computation.31 | convolution fusion | flops 4320657408 | bytes 15728640 | tf_op jit(solution)/shard_map/dot_general | solution.py:35
  55.1 0.0 copy-done.1
  55.1 0.5 fusion.21
  55.6 20.5 %all-gather.2 = f32[8,1,256]{2,1,0:T(1,128)S(1)} all-gather(f32[1,1,256]{2,1,0:T(1,128)S(1)} %bitcast.56), channel_id=2, replica_groups=mesh['sp'=8,'tp'=4] {'sp'}, dimensions={0}, use_global_device_ids=true | all-gather | bytes 9216 | tf_op jit(solution)/shard_map/all_gather | solution.py:16
  76.1 0.3 while.12
  76.5 0.2 reshape.30
  76.7 0.3 copy.11
  76.9 0.1 fusion.23
  77.2 0.3 copy.12
  77.5 0.2 fusion.14
  77.6 0.9 fusion.24
  78.6 0.0 all-gather.8.cloned.1.call-update
  78.6 36.8 %all-gather.8.cloned.1.call-done = f32[32,64,128]{2,1,0:T(8,128)} async-done(((f32[4,64,128]{2,1,0:T(8,128)}), f32[32,64,128]{2,1,0:T(8,128)}) %all-gather.8.cloned.1.call-update) | async-done | bytes 1048592 | tf_op jit(solution)/shard_map/all_gather | solution.py:59
  115.4 1.3 %reduce_sum.28 = f32[4,64,128]{2,1,0:T(8,128)S(1)} reduce(f32[8,4,64,128]{3,2,1,0:T(8,128)} %bitcast.50, f32[]{:T(128)} %constant.48.clone.1), dimensions={0}, to_apply=%region_5.6 | reduce | flops 229376 | bytes 1179652 | tf_op jit(solution)/shard_map/reduce_sum | solution.py:59
  116.7 0.0 copy-done
  116.7 0.2 fusion.17
  116.9 0.1 multiply_reduce_fusion
  117.0 0.6 multiply_convert_fusion
  117.6 0.6 dynamic-slice_convert_fusion
  (24 shorter events, 0.3 us)
Async XLA Ops:
  7.2 109.5 %copy-start = (bf16[4,64]{1,0:T(4,128)(2,1)S(1)}, bf16[4,64]{1,0:T(4,128)(2,1)}, u32[]{:S(2)}) copy-start(bf16[4,64]{1,0:T(4,128)(2,1)} %param.13) | copy-start | bytes 1540
  7.2 39.6 %all-gather.6.cloned.1.call-start = ((), (), s32[]{:S(2)}) async-start(), calls=%async_computation | async-start | bytes 5242880 | tf_op jit(solution)/shard_map/all_gather | solution.py:36
  7.9 107.5 %all-gather.8.cloned.1.call-start = ((), (), s32[]{:S(2)}) async-start(), calls=%async_computation.1 | async-start | bytes 1179648 | tf_op jit(solution)/shard_map/all_gather | solution.py:59
  8.0 47.1 %copy-start.1 = (f32[256]{0:T(256)S(1)}, f32[256]{0:T(256)}, u32[]{:S(2)}) copy-start(f32[256]{0:T(256)} %param.12) | copy-start | bytes 3076
Sparse Core Ops, SparseCore 0:
  9.5 37.1 all-gather.5
  78.7 36.5 all-gather.7
